TPU v7x, 32 devices: a whole 2x2x4 slice. The times are simulated.
32 devices in a mesh: sp: 8 (over z, y), tp: 4 (over x, core).
Axes of the slice: x: 2, y: 2, z: 4, core: 2. Of those that a mesh axis runs over, the one named last changes fastest.
Arguments:
- middle_stream: bfloat16 [1536, 2048], P('sp', 'tp'), may hold values from -6 to 6
- output_gradient: bfloat16 [1536, 2048], P('sp', 'tp'), may hold values from -6 to 6
- routes: int32 [1536, 2], P('sp'), may hold values from 0 to 7, all different within a row; in each aligned block of 192 rows (0 to 191, 192 to 383, ...) at most 72 rows name the same one
- chosen_expert_weight: float32 [1536, 2], P('sp'), may hold values from 0.2 to 1
- expert_gate_weight: bfloat16 [8, 2048, 3584], P('sp', None, 'tp'), may hold values from -0.125 to 0.125
- expert_up_weight: bfloat16 [8, 2048, 3584], P('sp', None, 'tp'), may hold values from -0.125 to 0.125
- expert_down_weight: bfloat16 [8, 3584, 2048], P('sp', 'tp'), may hold values from -0.09375 to 0.09375
- recurrent_output_weight: bfloat16 [2048, 1024], P(None, 'tp'), may hold values from -0.1875 to 0.1875
- recurrence_input: bfloat16 [1536, 1024], P('sp', 'tp'), may hold values from -8 to 8
- output_gate_logits: bfloat16 [1536, 1024], P('sp', 'tp'), may hold values from -6 to 6
- recurrence_gate_weight: bfloat16 [8, 128, 128], replicated, may hold values from -0.5 to 0.5
- input_gate_weight: bfloat16 [8, 128, 128], replicated, may hold values from -0.5 to 0.5
- channel_decay_param: float32 [1024], P('tp'), may hold values from 4 to 13
- extra_log_decay: float32 [1536, 1024], P('sp', 'tp'), may hold values from -0.7 to 0
Outputs:
- grad_gate: bfloat16 [8, 2048, 3584], P('sp', None, 'tp')
- grad_up: bfloat16 [8, 2048, 3584], P('sp', None, 'tp')
- grad_down: bfloat16 [8, 3584, 2048], P('sp', 'tp')
- grad_out_proj: float32 [2048, 1024], P('sp', 'tp')
- grad_input: float32 [1536, 1024], P('sp', 'tp')
- grad_gate_pre: float32 [1536, 1024], P('sp', 'tp')
Inputs may be any that keep to these rules, and one draw needn't show every extreme that they name: `routes`: in the rows of one index of sp no expert is named more than 72 times, a bound that some block reaches in some of them; the entries of a row differ.
All inputs are finite; a program needn't handle non-finite values.
Results may differ from a plain program's by a relative error of at most 0.017.
Values may be sent and summed in bfloat16 or wider, within the bound.
A program may use at most 128 MiB of HBM per device.

v0:
```python
import functools

import jax
import jax.numpy as jnp
from jax import lax
from jax.experimental import pallas as pl
from jax.experimental.pallas import tpu as pltpu
from jax.sharding import PartitionSpec as P

MESH = pl.DeviceIdType.MESH


def partner(t, stage, m):
    d = m >> (stage + 1)
    return t + d * (1 - 2 * ((t // d) % 2))


def flipped(s, j, n):
    out = 0
    for b in range(n.bit_length() - 1):
        bit = (s // 2**b) % 2
        out = out + (1 - bit if (j >> b) % 2 else bit) * 2**b
    return out


def far_near(n):
    near, far = list(range(n // 2)), list(range(n // 2, n))
    arrive = near[:1]
    for i in range(1, n // 2):
        arrive += [near[i], far[i - 1]]
    leave = []
    for i in range(1, n // 2):
        leave += [far[i - 1], near[i]]
    return arrive + far[-1:], leave + far[-1:], far + near[1:] + near[:1]


def held_columns(t, stage, m):
    if stage == 0:
        return [t]
    return held_columns(t, stage - 1, m) + held_columns(partner(t, stage - 1, m), stage - 1, m)


def greet(peers):
    barrier = pltpu.get_barrier_semaphore()
    for peer in peers:
        pl.semaphore_signal(barrier, inc=1, device_id=peer, device_id_type=MESH)
    pl.semaphore_wait(barrier, len(peers))


def remote(src, dst, send_sem, recv_sem, peer):
    return pltpu.make_async_remote_copy(
        src_ref=src,
        dst_ref=dst,
        send_sem=send_sem,
        recv_sem=recv_sem,
        device_id=peer,
        device_id_type=MESH,
    )


def shifted(value, k, fill, reverse):
    pad = jnp.full((k, value.shape[1]), fill, value.dtype)
    if reverse:
        return jnp.concatenate([value[k:], pad], axis=0)
    return jnp.concatenate([pad, value[:-k]], axis=0)


def local_scan(gain, term, reverse):
    k = 1
    while k < gain.shape[0]:
        term = term + gain * shifted(term, k, 0.0, reverse)
        gain = gain * shifted(gain, k, 1.0, reverse)
        k *= 2
    return gain, term


def dispatch_kernel(
    n,
    m,
    rows_ref,
    cot_ref,
    decay_ref,
    driven_ref,
    rows_out,
    cot_out,
    states_ref,
    prev_ref,
    gain_buf,
    car_send,
    car_buf,
    a2a_send,
    a2a_recv,
    tp_send,
    tp_recv,
    car_ssem,
    car_rsem,
    self_sem,
):
    sources, targets = (rows_ref, cot_ref), (rows_out, cot_out)
    s, t = lax.axis_index("sp"), lax.axis_index("tp")
    feat = rows_ref.shape[2]
    stages = m.bit_length() - 1
    greet(
        [{"sp": lax.rem(s + k, n)} for k in range(1, n)]
        + [{"tp": partner(t, j, m)} for j in range(stages)]
    )

    def block(a, src, col):
        return targets[a].at[src, :, pl.ds(pl.multiple_of(col * feat, feat), feat)]

    first = {}
    arrive, leave, _ = far_near(n)
    for k in [0] + leave:
        dst = flipped(s, k, n)
        for a in range(2):
            if k == 0:
                copy = pltpu.make_async_copy(sources[a].at[s], block(a, s, t), self_sem.at[a])
            else:
                copy = remote(
                    sources[a].at[dst],
                    block(a, s, t),
                    a2a_send.at[a, k],
                    a2a_recv.at[a, k],
                    {"sp": dst},
                )
            copy.start()
            first[k, a] = copy

    pushed = []

    def push(a, k, stage, i, col):
        src = flipped(s, k, n)
        at = 2**stage - 1 + i
        copy = remote(
            block(a, src, col),
            block(a, src, col),
            tp_send.at[a, at, k],
            tp_recv.at[a, at, k],
            {"tp": partner(t, stage, m)},
        )
        copy.start()
        pushed.append(copy)

    def arrived(k, stage):
        src = flipped(s, k, n)
        cols = held_columns(partner(t, stage, m), stage, m)
        for i, col in enumerate(cols):
            at = 2**stage - 1 + i
            for a in range(2):
                remote(
                    block(a, src, col),
                    block(a, src, col),
                    tp_send.at[a, at, k],
                    tp_recv.at[a, at, k],
                    {"tp": partner(t, stage, m)},
                ).wait_recv()
                for later in range(stage + 1, stages):
                    push(a, k, later, 2**stage + i, col)

    def forward(k):
        for a in range(2):
            if k == 0:
                first[k, a].wait()
            else:
                first[k, a].wait_recv()
            for stage in range(stages):
                push(a, k, stage, 0, t)

    forward(arrive[0])
    gain, term = local_scan(decay_ref[...], driven_ref[...], False)
    gain_buf[...] = gain
    states_ref[...] = term
    rows = gain.shape[0]
    car_send[0:1] = gain[rows - 1 : rows]
    car_send[1:2] = term[rows - 1 : rows]
    forward(arrive[1])
    carries = []
    for k in range(1, n):
        copy = remote(
            car_send, car_buf.at[k], car_ssem.at[k], car_rsem.at[k], {"sp": lax.rem(s + k, n)}
        )
        copy.start()
        carries.append(copy)
    for at in range(2, n):
        forward(arrive[at])
        for stage in range(stages - 1):
            arrived(arrive[at - 2], stage)
    for copy in carries:
        copy.wait()
    carry = jnp.zeros((1, gain_buf.shape[1]), jnp.float32)
    for k in range(n - 1, 0, -1):
        carry = jnp.where(k <= s, car_buf[k, 0:1] * carry + car_buf[k, 1:2], carry)
    states = states_ref[...] + gain_buf[...] * carry
    states_ref[...] = states
    prev_ref[...] = jnp.concatenate([carry, states[:-1]], axis=0)
    for k in arrive[n - 2 :]:
        for stage in range(stages - 1):
            arrived(k, stage)
    for k in range(n):
        arrived(k, stages - 1)
    for k in leave:
        for a in range(2):
            first[k, a].wait_send()
    for copy in pushed:
        copy.wait_send()


def dispatch(send_rows, send_cot, decay, driven):
    n, m = lax.axis_size("sp"), lax.axis_size("tp")
    _, cap, feat = send_rows.shape
    whole = jax.ShapeDtypeStruct((n, cap, m * feat), send_rows.dtype)
    rows, channels = decay.shape
    vmem = pl.BlockSpec(memory_space=pltpu.VMEM)
    state = jax.ShapeDtypeStruct((rows, channels), jnp.float32)
    return pl.pallas_call(
        functools.partial(dispatch_kernel, n, m),
        out_shape=(whole, whole, state, state),
        in_specs=[vmem] * 4,
        out_specs=(vmem,) * 4,
        scratch_shapes=[
            pltpu.VMEM((rows, channels), jnp.float32),
            pltpu.VMEM((2, channels), jnp.float32),
            pltpu.VMEM((n, 2, channels), jnp.float32),
            pltpu.SemaphoreType.DMA((2, n)),
            pltpu.SemaphoreType.DMA((2, n)),
            pltpu.SemaphoreType.DMA((2, m - 1, n)),
            pltpu.SemaphoreType.DMA((2, m - 1, n)),
            pltpu.SemaphoreType.DMA((n,)),
            pltpu.SemaphoreType.DMA((n,)),
            pltpu.SemaphoreType.DMA((2,)),
        ],
        compiler_params=pltpu.CompilerParams(collective_id=0, has_side_effects=True),
        name="dispatch",
    )(send_rows, send_cot, decay, driven)


def return_kernel(
    n,
    m,
    part_ref,
    pick_ref,
    cot_ref,
    out_ref,
    in_buf,
    acc_buf,
    back_buf,
    rs_send,
    rs_recv,
    a2a_send,
    a2a_recv,
    ag_send,
    ag_recv,
):
    s, t = lax.axis_index("sp"), lax.axis_index("tp")
    feat = cot_ref.shape[1]
    stages = m.bit_length() - 1

    def across(stage):
        d = 2**stage
        return t + d * (1 - 2 * ((t // d) % 2))

    greet(
        [{"sp": lax.rem(s + k, n)} for k in range(1, n)] + [{"tp": across(j)} for j in range(stages)]
    )

    def cols(col):
        return pl.ds(pl.multiple_of(col * feat, feat), feat)

    base = []
    total = 0
    for stage in range(stages):
        base.append(total)
        total += m >> (stage + 1)

    order = far_near(n)[2]
    waits = []

    def send_stage(k, stage):
        dst = flipped(s, k, n)
        source = part_ref if stage == 0 else acc_buf
        peer = across(stage)
        step = 2 ** (stage + 1)
        for i in range(m // step):
            col = lax.rem(peer + i * step, m)
            at = base[stage] + i
            copy = remote(
                source.at[dst, :, cols(col)],
                in_buf.at[at, k],
                rs_send.at[at, k],
                rs_recv.at[at, k],
                {"tp": peer},
            )
            copy.start()
            waits.append(copy)

    def sum_stage(k, stage):
        dst = flipped(s, k, n)
        source = part_ref if stage == 0 else acc_buf
        step = 2 ** (stage + 1)
        for i in range(m // step):
            col = lax.rem(t + i * step, m)
            at = base[stage] + i
            remote(
                source.at[dst, :, cols(col)],
                in_buf.at[at, k],
                rs_send.at[at, k],
                rs_recv.at[at, k],
                {"tp": across(stage)},
            ).wait_recv()
            mine = source[dst, :, cols(col)].astype(jnp.float32)
            acc_buf[dst, :, cols(col)] = (mine + in_buf[at, k].astype(jnp.float32)).astype(
                jnp.bfloat16
            )

    def send_home(k):
        dst = flipped(s, k, n)
        if k == 0:
            back_buf[s] = acc_buf[s, :, cols(t)]
            return
        copy = remote(
            acc_buf.at[dst, :, cols(t)],
            back_buf.at[s],
            a2a_send.at[k],
            a2a_recv.at[k],
            {"sp": dst},
        )
        copy.start()
        waits.append(copy)

    for k in order:
        send_stage(k, 0)
    for at in range(n + stages - 1):
        for stage in range(stages):
            if 0 <= at - stage < n:
                k = order[at - stage]
                sum_stage(k, stage)
                if stage + 1 < stages:
                    send_stage(k, stage + 1)
                else:
                    send_home(k)
    value = cot_ref[...].astype(jnp.float32)
    for k in [0] + order[:-1]:
        src = flipped(s, k, n)
        if k > 0:
            remote(
                acc_buf.at[src, :, cols(t)],
                back_buf.at[src],
                a2a_send.at[k],
                a2a_recv.at[k],
                {"sp": src},
            ).wait_recv()
        value = value + jnp.dot(
            pick_ref[src], back_buf[src], preferred_element_type=jnp.float32
        )
    out_ref[:, cols(t)] = value.astype(jnp.bfloat16)

    def share(stage, i, col):
        at = 2**stage - 1 + i
        return remote(
            out_ref.at[:, cols(col)],
            out_ref.at[:, cols(col)],
            ag_send.at[at],
            ag_recv.at[at],
            {"tp": partner(t, stage, m)},
        )

    def push(stage, i, col):
        copy = share(stage, i, col)
        copy.start()
        waits.append(copy)

    for stage in range(stages):
        push(stage, 0, t)
    for stage in range(stages):
        for i, col in enumerate(held_columns(partner(t, stage, m), stage, m)):
            share(stage, i, col).wait_recv()
            for later in range(stage + 1, stages):
                push(later, 2**stage + i, col)
    for copy in waits:
        copy.wait_send()


def bring_back(part, pick, output_gradient):
    n, m = lax.axis_size("sp"), lax.axis_size("tp")
    _, cap, width = part.shape
    rows, feat = output_gradient.shape
    vmem = pl.BlockSpec(memory_space=pltpu.VMEM)
    return pl.pallas_call(
        functools.partial(return_kernel, n, m),
        out_shape=jax.ShapeDtypeStruct((rows, width), jnp.bfloat16),
        in_specs=[vmem] * 3,
        out_specs=vmem,
        scratch_shapes=[
            pltpu.VMEM((m - 1, n, cap, feat), jnp.bfloat16),
            pltpu.VMEM((n, cap, width), jnp.bfloat16),
            pltpu.VMEM((n, cap, feat), jnp.bfloat16),
            pltpu.SemaphoreType.DMA((m - 1, n)),
            pltpu.SemaphoreType.DMA((m - 1, n)),
            pltpu.SemaphoreType.DMA((n,)),
            pltpu.SemaphoreType.DMA((n,)),
            pltpu.SemaphoreType.DMA((m - 1,)),
            pltpu.SemaphoreType.DMA((m - 1,)),
        ],
        compiler_params=pltpu.CompilerParams(collective_id=2, has_side_effects=True),
        name="bring_back",
    )(part, pick, output_gradient)


def tail_kernel(
    n,
    decay_ref,
    input_ref,
    part_ref,
    grad_ref,
    sum_ref,
    gain_buf,
    car_send,
    car_buf,
    part_buf,
    pair_buf,
    part_ssem,
    part_rsem,
    car_ssem,
    car_rsem,
):
    s = lax.axis_index("sp")
    greet([{"sp": lax.rem(s + k, n)} for k in range(1, n)])
    beside = flipped(s, 1, n)
    half = n // 2
    order = [half - 1 - j for j in range(half)]
    near = {}
    for j in order:
        dst = flipped(s, 2 * j + 1, n)
        near[j] = remote(
            part_ref.at[dst], part_buf.at[j], part_ssem.at[j], part_rsem.at[j], {"sp": beside}
        )
        near[j].start()
    decay = decay_ref[...]
    gain, term = local_scan(shifted(decay, 1, 1.0, True), input_ref[...], True)
    gain_buf[...] = gain
    grad_ref[...] = term
    car_send[0:1] = decay[0:1] * gain[0:1]
    car_send[1:2] = decay[0:1] * term[0:1]
    carries = []
    for k in range(1, n):
        copy = remote(
            car_send, car_buf.at[k], car_ssem.at[k], car_rsem.at[k], {"sp": lax.rem(s + k, n)}
        )
        copy.start()
        carries.append(copy)
    far = {}
    for j in order:
        near[j].wait_recv()
        home = flipped(s, 2 * j, n)
        both = part_ref[home].astype(jnp.float32) + part_buf[j].astype(jnp.float32)
        if j == 0:
            sum_ref[...] = both
            continue
        pair_buf[j] = both.astype(jnp.bfloat16)
        at = half + j
        far[j] = remote(
            pair_buf.at[j], part_buf.at[at], part_ssem.at[at], part_rsem.at[at], {"sp": home}
        )
        far[j].start()
    for copy in carries:
        copy.wait()
    carry = jnp.zeros((1, gain_buf.shape[1]), jnp.float32)
    for k in range(1, n):
        carry = jnp.where(k > s, car_buf[k, 0:1] * carry + car_buf[k, 1:2], carry)
    grad_ref[...] = grad_ref[...] + gain_buf[...] * carry
    for j in order[:-1]:
        far[j].wait_recv()
        sum_ref[...] += part_buf[half + j].astype(jnp.float32)
    for j in order:
        near[j].wait_send()
    for j in order[:-1]:
        far[j].wait_send()


def tail(decay, state_in, part):
    n = lax.axis_size("sp")
    rows, channels = decay.shape
    vmem = pl.BlockSpec(memory_space=pltpu.VMEM)
    return pl.pallas_call(
        functools.partial(tail_kernel, n),
        out_shape=(
            jax.ShapeDtypeStruct((rows, channels), jnp.float32),
            jax.ShapeDtypeStruct(part.shape[1:], jnp.float32),
        ),
        in_specs=[vmem] * 3,
        out_specs=(vmem,) * 2,
        scratch_shapes=[
            pltpu.VMEM((rows, channels), jnp.float32),
            pltpu.VMEM((2, channels), jnp.float32),
            pltpu.VMEM((n, 2, channels), jnp.float32),
            pltpu.VMEM(part.shape, part.dtype),
            pltpu.VMEM((n // 2,) + part.shape[1:], part.dtype),
            pltpu.SemaphoreType.DMA((n,)),
            pltpu.SemaphoreType.DMA((n,)),
            pltpu.SemaphoreType.DMA((n,)),
            pltpu.SemaphoreType.DMA((n,)),
        ],
        compiler_params=pltpu.CompilerParams(collective_id=1, has_side_effects=True),
        name="tail",
    )(decay, state_in, part)


def gelu_parts(output_gate_logits):
    gate_float = output_gate_logits.astype(jnp.float32)
    return jax.jvp(jax.nn.gelu, (gate_float,), (jnp.ones_like(gate_float),))


def expert_backward(inputs, cotangent, gate_weight, up_weight, down_weight):
    gate_act = jnp.dot(inputs, gate_weight, preferred_element_type=jnp.float32)
    up_act = jnp.dot(inputs, up_weight, preferred_element_type=jnp.float32)
    sigmoid_gate = jax.nn.sigmoid(gate_act)
    silu_act = gate_act * sigmoid_gate
    hidden = (silu_act * up_act).astype(jnp.bfloat16)
    d_hidden = lax.dot_general(
        cotangent, down_weight, (((1,), (1,)), ((), ())), preferred_element_type=jnp.float32
    )
    grad_down = lax.dot_general(
        hidden, cotangent, (((0,), (0,)), ((), ())), preferred_element_type=jnp.float32
    )
    d_gate = (d_hidden * up_act * sigmoid_gate * (1.0 + gate_act * (1.0 - sigmoid_gate))).astype(
        jnp.bfloat16
    )
    d_up = (d_hidden * silu_act).astype(jnp.bfloat16)
    grad_gate = lax.dot_general(
        inputs, d_gate, (((0,), (0,)), ((), ())), preferred_element_type=jnp.float32
    )
    grad_up = lax.dot_general(
        inputs, d_up, (((0,), (0,)), ((), ())), preferred_element_type=jnp.float32
    )
    partial_value = lax.dot_general(
        d_gate, gate_weight, (((1,), (1,)), ((), ())), preferred_element_type=jnp.float32
    )
    partial_value = partial_value + lax.dot_general(
        d_up, up_weight, (((1,), (1,)), ((), ())), preferred_element_type=jnp.float32
    )
    return (
        grad_gate.astype(jnp.bfloat16),
        grad_up.astype(jnp.bfloat16),
        grad_down.astype(jnp.bfloat16),
        partial_value,
    )


def per_device(
    middle_stream,
    output_gradient,
    routes,
    chosen_expert_weight,
    expert_gate_weight,
    expert_up_weight,
    expert_down_weight,
    recurrent_output_weight,
    recurrence_input,
    output_gate_logits,
    recurrence_gate_weight,
    input_gate_weight,
    channel_decay_param,
    extra_log_decay,
):
    rows_dev = middle_stream.shape[0]
    top_count = routes.shape[1]
    experts = lax.axis_size("sp")
    capacity = 3 * top_count * rows_dev // (2 * experts)
    feat_width = middle_stream.shape[1]
    choice = routes.T
    expert_ids = jnp.arange(experts, dtype=jnp.int32)
    named = [(choice[k][None, :] == expert_ids[:, None]) for k in range(top_count)]
    named_any = sum(part.astype(jnp.bfloat16) for part in named)
    position = jnp.arange(rows_dev, dtype=jnp.int32)
    earlier = (position[:, None] < position[None, :]).astype(jnp.bfloat16)
    rank = jnp.dot(named_any, earlier, preferred_element_type=jnp.float32).astype(jnp.int32)
    slot_ids = jnp.arange(experts * capacity, dtype=jnp.int32)
    picks = []
    for k in range(top_count):
        slot = jnp.sum(
            jnp.where(named[k], rank + expert_ids[:, None] * capacity, 0), axis=0, keepdims=True
        )
        picks.append((slot_ids[:, None] == slot).astype(jnp.bfloat16))
    pick_any = sum(picks)
    pick_both = jnp.concatenate(picks, axis=1)
    pair_cot = (
        chosen_expert_weight.T[:, :, None] * output_gradient.astype(jnp.float32)[None]
    ).astype(jnp.bfloat16)
    pair_cot = pair_cot.reshape(-1, feat_width)
    send_rows = jnp.dot(pick_any, middle_stream, preferred_element_type=jnp.bfloat16)
    send_cot = jnp.dot(pick_both, pair_cot, preferred_element_type=jnp.bfloat16)
    channels = recurrence_input.shape[1]
    block_width = recurrence_gate_weight.shape[1]
    local_blocks = channels // block_width
    first_block = lax.axis_index("tp") * local_blocks
    recall_weight = lax.dynamic_slice_in_dim(recurrence_gate_weight, first_block, local_blocks, 0)
    admit_weight = lax.dynamic_slice_in_dim(input_gate_weight, first_block, local_blocks, 0)
    u_blocks = recurrence_input.reshape(rows_dev, local_blocks, block_width)
    forget_gate = jax.nn.sigmoid(
        jnp.einsum(
            "tnb,nbc->tnc", u_blocks, recall_weight, preferred_element_type=jnp.float32
        ).reshape(rows_dev, channels)
    )
    admit_gate = jax.nn.sigmoid(
        jnp.einsum(
            "tnb,nbc->tnc", u_blocks, admit_weight, preferred_element_type=jnp.float32
        ).reshape(rows_dev, channels)
    )
    baseline_rate = jax.nn.softplus(-channel_decay_param)
    decay_logarithm = -8.0 * forget_gate * baseline_rate[None, :] + extra_log_decay
    decay_step = jnp.exp(decay_logarithm)
    input_scale = jnp.sqrt(-jnp.expm1(2.0 * decay_logarithm))
    u_float = recurrence_input.astype(jnp.float32)
    driven = u_float * admit_gate * input_scale
    recv_rows, recv_cot, states, prev_states = dispatch(
        send_rows.reshape(experts, capacity, feat_width),
        send_cot.reshape(experts, capacity, feat_width),
        decay_step,
        driven,
    )
    row_width = recv_rows.shape[2]
    inputs = recv_rows.reshape(-1, row_width)
    cotangent = recv_cot.reshape(-1, row_width)
    grad_gate, grad_up, grad_down, partial_value = expert_backward(
        inputs, cotangent, expert_gate_weight[0], expert_up_weight[0], expert_down_weight[0]
    )
    grad_full = bring_back(
        partial_value.astype(jnp.bfloat16).reshape(experts, capacity, row_width),
        pick_any.reshape(experts, capacity, rows_dev).transpose(0, 2, 1),
        output_gradient,
    )
    mixer_grad = jnp.dot(grad_full, recurrent_output_weight, preferred_element_type=jnp.float32)
    gelu_val, gelu_der = gelu_parts(output_gate_logits)
    lru_out = (states * gelu_val).astype(jnp.bfloat16)
    gop_part = lax.dot_general(
        grad_full, lru_out, (((0,), (0,)), ((), ())), preferred_element_type=jnp.float32
    ).astype(jnp.bfloat16)
    gop_part = gop_part.reshape(experts, -1, channels)
    grad_gate_pre = mixer_grad * states * gelu_der
    state_in = mixer_grad * gelu_val
    state_grad, grad_out_proj = tail(decay_step, state_in, gop_part)
    d_log = state_grad * (
        prev_states * decay_step - u_float * admit_gate * decay_step * decay_step / input_scale
    )
    d_recall = (d_log * (-8.0 * baseline_rate[None, :]) * forget_gate * (1.0 - forget_gate)).astype(
        jnp.bfloat16
    )
    d_admit = (state_grad * u_float * input_scale * admit_gate * (1.0 - admit_gate)).astype(
        jnp.bfloat16
    )
    back_recall = jnp.einsum(
        "tnc,nbc->tnb",
        d_recall.reshape(rows_dev, local_blocks, block_width),
        recall_weight,
        preferred_element_type=jnp.float32,
    )
    back_admit = jnp.einsum(
        "tnc,nbc->tnb",
        d_admit.reshape(rows_dev, local_blocks, block_width),
        admit_weight,
        preferred_element_type=jnp.float32,
    )
    grad_input = state_grad * admit_gate * input_scale + (back_recall + back_admit).reshape(
        rows_dev, channels
    )
    return (
        grad_gate[None],
        grad_up[None],
        grad_down[None],
        grad_out_proj,
        grad_input,
        grad_gate_pre,
    )


def solution(mesh):
    placed = (
        P("sp", "tp"),
        P("sp", "tp"),
        P("sp", None),
        P("sp", None),
        P("sp", None, "tp"),
        P("sp", None, "tp"),
        P("sp", "tp", None),
        P(None, "tp"),
        P("sp", "tp"),
        P("sp", "tp"),
        P(),
        P(),
        P("tp"),
        P("sp", "tp"),
    )
    return jax.shard_map(
        per_device,
        mesh=mesh,
        in_specs=placed,
        out_specs=(
            P("sp", None, "tp"),
            P("sp", None, "tp"),
            P("sp", "tp", None),
            P("sp", "tp"),
            P("sp", "tp"),
            P("sp", "tp"),
        ),
        check_vma=False,
    )
```

profile of v0, /device:TPU:1, one launch (start us, length us, event | category | flops | bytes accessed | tf_op | source)
XLA Modules:
  0.0 153.6 jit_solution(5859017065044662931)
XLA Ops:
  0.7 1.2 fusion.17
  1.9 1.1 fusion.21
  3.0 0.7 fusion.90
  3.7 1.8 %fusion.63 = (f32[192,256]{1,0:T(8,128)}, f32[192,256]{1,0:T(8,128)S(1)}) fusion(f32[2,24,8,128]{3,2,1,0:T(8,128)S(1)} %fusion.17, bf16[192,256]{1,0:T(8,128)(2,1)} %param.22, f32[192,256]{1,0:T(8,128)} %param.27, f32[256]{0:T(256)S(1)} %fusion.90, f32[2,24,8,128]{3,2,1,0:T(8,128)S(1)} %fusion.21), kind=kLoop, calls=%fused_computation.94 | loop fusion | flops 344064 | bytes 1082368 | tf_op jit(solution)/shard_map/mul | solution.py:614
  5.5 0.7 exp.22.decay_ref
  6.2 0.2 select_reduce_fusion.1
  6.4 0.2 broadcast_compare_fusion.1
  6.7 0.1 mul.170
  6.8 0.1 fusion.27
  6.9 1.3 fusion.23.cot_ref
  8.3 1.1 fusion.34
  9.4 43.1 %dispatch.1 = (bf16[8,72,2048]{2,1,0:T(8,128)(2,1)}, bf16[8,72,2048]{2,1,0:T(8,128)(2,1)}, f32[192,256]{1,0:T(8,128)}, f32[192,256]{1,0:T(8,128)}) custom-call(bf16[8,72,512]{2,1,0:T(8,128)(2,1)} %bitcast.120, bf16[8,72,512]{2,1,0:T(8,128)(2,1)} %fusion.23.cot_ref, f32[192,256]{1,0:T(8,128)} %exp.22.decay_ref, f32[192,256]{1,0:T(8,128)} %get-tuple-element.20.driven_ref), custom_call_target="tpu_custom_call" | custom-call | tf_op jit(solution)/shard_map/dispatch/pallas_call | solution.py:215
  52.5 5.5 %fusion.2 = f32[576,896]{1,0:T(8,128)S(1)} fusion(bf16[576,2048]{1,0:T(8,128)(2,1)} %bitcast.125, bf16[1,2048,896]{2,1,0:T(8,128)(2,1)} %param.18), kind=kOutput, calls=%fused_computation.3 | convolution fusion | flops 2113929216 | bytes 8093696 | tf_op jit(solution)/shard_map/dot_general | solution.py:514
  58.1 2.6 %fusion.6 = f32[576,896]{1,0:T(8,128)S(1)} fusion(bf16[576,2048]{1,0:T(8,128)(2,1)S(1)} %bitcast.126, bf16[1,2048,896]{2,1,0:T(8,128)(2,1)S(1)} %copy-done.9), kind=kOutput, calls=%fused_computation.7 | convolution fusion | flops 2113929216 | bytes 8093696 | tf_op jit(solution)/shard_map/dot_general | solution.py:515
  60.7 0.1 copy-done.7
  60.8 0.7 copy-done.12
  61.6 3.2 %multiply_convert_fusion.1 = (bf16[576,896]{1,0:T(8,128)(2,1)S(1)}, bf16[576,896]{1,0:T(8,128)(2,1)S(1)}) fusion(f32[576,896]{1,0:T(8,128)S(1)} %fusion.2, f32[576,896]{1,0:T(8,128)S(1)} %fusion.6, bf16[576,2048]{1,0:T(8,128)(2,1)S(1)} %bitcast.129, bf16[1,896,2048]{2,1,0:T(8,128)(2,1)S(1)} %copy-done.7), kind=kOutput, calls=%fused_computation.16 | convolution fusion | flops 2120638464 | bytes 12222464 | tf_op jit(solution)/shard_map/dot_general | solution.py:519
  64.8 2.6 %fusion = f32[576,2048]{1,0:T(8,128)S(1)} fusion(bf16[576,896]{1,0:T(8,128)(2,1)S(1)} %get-tuple-element.23, bf16[1,2048,896]{2,1,0:T(8,128)(2,1)S(1)} %copy-done.8), kind=kOutput, calls=%fused_computation.1 | convolution fusion | flops 2113929216 | bytes 9420800 | tf_op jit(solution)/shard_map/dot_general | solution.py:535
  67.5 3.9 %add_convert_fusion = bf16[576,2048]{1,0:T(8,128)(2,1)} fusion(f32[576,2048]{1,0:T(8,128)S(1)} %fusion, bf16[576,896]{1,0:T(8,128)(2,1)S(1)} %get-tuple-element.22, bf16[1,2048,896]{2,1,0:T(8,128)(2,1)S(1)} %copy-done.9), kind=kOutput, calls=%fused_computation | convolution fusion | flops 2116288512 | bytes 11780096 | tf_op jit(solution)/shard_map/dot_general | solution.py:538
  71.4 1.0 fusion.30.pick_ref
  72.4 32.3 %bring_back.1 = bf16[192,2048]{1,0:T(8,128)(2,1)} custom-call(bf16[8,72,2048]{2,1,0:T(8,128)(2,1)} %bitcast.118, bf16[8,192,72]{2,1,0:T(8,128)(2,1)} %fusion.30.pick_ref, bf16[192,512]{1,0:T(8,128)(2,1)} %cot_ref.1), custom_call_target="tpu_custom_call" | custom-call | tf_op jit(solution)/shard_map/bring_back/pallas_call | solution.py:388
  104.7 2.6 %convolution_convert_fusion = bf16[2048,256]{1,0:T(8,128)(2,1)} fusion(bf16[192,2048]{1,0:T(8,128)(2,1)} %bring_back.1, f32[192,256]{1,0:T(8,128)S(1)} %copy-done.15, bf16[192,256]{1,0:T(8,128)(2,1)S(1)} %copy-done.16), kind=kOutput, calls=%fused_computation.14 | convolution fusion | flops 202391552 | bytes 2129920 | tf_op jit(solution)/shard_map/dot_general | solution.py:635
  107.4 2.3 %fusion.58 = (f32[192,256]{1,0:T(8,128)}, f32[192,256]{1,0:T(8,128)}) fusion(bf16[192,256]{1,0:T(8,128)(2,1)S(1)} %copy-done.16, f32[192,256]{1,0:T(8,128)S(1)} %copy-done.15, bf16[192,2048]{1,0:T(8,128)(2,1)} %bring_back.1, bf16[2048,256]{1,0:T(8,128)(2,1)S(1)} %copy-done), kind=kOutput, calls=%fused_computation.81 | convolution fusion | flops 202358784 | bytes 2523136 | tf_op jit(solution)/shard_map/dot_general | solution.py:632
  109.7 21.2 %tail.1 = (f32[192,256]{1,0:T(8,128)}, f32[256,256]{1,0:T(8,128)}) custom-call(f32[192,256]{1,0:T(8,128)} %exp.22.decay_ref, f32[192,256]{1,0:T(8,128)} %get-tuple-element.27.input_ref, bf16[8,256,256]{2,1,0:T(8,128)(2,1)} %bitcast.119), custom_call_target="tpu_custom_call" | custom-call | tf_op jit(solution)/shard_map/tail/pallas_call | solution.py:484
  131.0 1.3 fusion.64
  132.3 1.0 fusion.67
  133.4 1.0 fusion.13
  134.4 1.7 %bitcast_add_fusion = f32[192,256]{1,0:T(8,128)} fusion(f32[2,24,8,128]{3,2,1,0:T(8,128)S(1)} %fusion.13, f32[192,256]{1,0:T(8,128)} %get-tuple-element.16, f32[2,24,8,128]{3,2,1,0:T(8,128)S(1)} %fusion.17, f32[192,256]{1,0:T(8,128)S(1)} %get-tuple-element.21), kind=kLoop, calls=%fused_computation.82 | loop fusion | flops 245760 | bytes 983040 | tf_op jit(solution)/shard_map/add | solution.py:663
  136.1 7.0 %convert_bitcast_fusion = bf16[1,896,2048]{2,1,0:T(8,128)(2,1)} fusion(bf16[576,2048]{1,0:T(8,128)(2,1)S(1)} %bitcast.130, f32[576,896]{1,0:T(8,128)} %copy-done.18, f32[576,896]{1,0:T(8,128)} %copy-done.17), kind=kOutput, calls=%fused_computation.11 | convolution fusion | flops 2118860800 | bytes 10158080 | tf_op jit(solution)/shard_map/dot_general | solution.py:522
  143.2 4.8 %convert_bitcast_fusion.1 = bf16[1,2048,896]{2,1,0:T(8,128)(2,1)} fusion(bf16[576,2048]{1,0:T(8,128)(2,1)S(1)} %bitcast.127, bf16[576,896]{1,0:T(8,128)(2,1)S(1)} %copy-done.20), kind=kOutput, calls=%fused_computation.12 | convolution fusion | flops 2115764224 | bytes 7061504 | tf_op jit(solution)/shard_map/dot_general | solution.py:532
  148.0 4.8 %convert_bitcast_fusion.2 = bf16[1,2048,896]{2,1,0:T(8,128)(2,1)} fusion(bf16[576,2048]{1,0:T(8,128)(2,1)S(1)} %bitcast.128, bf16[576,896]{1,0:T(8,128)(2,1)S(1)} %get-tuple-element.23), kind=kOutput, calls=%fused_computation.13 | convolution fusion | flops 2115764224 | bytes 7061504 | tf_op jit(solution)/shard_map/dot_general | solution.py:529
  152.8 0.7 copy.67
  (44 shorter events, 0.1 us)
Async XLA Ops:
  0.6 106.8 %copy-start = (bf16[2048,256]{1,0:T(8,128)(2,1)S(1)}, bf16[2048,256]{1,0:T(8,128)(2,1)}, u32[]{:S(2)}) copy-start(bf16[2048,256]{1,0:T(8,128)(2,1)} %param.21) | copy-start | bytes 3145732
  0.6 5.6 %copy-start.5 = (s32[192,2]{0,1:T(2,128)S(1)}, s32[192,2]{0,1:T(2,128)}, u32[]{:S(2)}) copy-start(s32[192,2]{0,1:T(2,128)} %param.16) | copy-start | bytes 4612
  0.7 6.0 %copy-start.1 = (bf16[192,512]{1,0:T(8,128)(2,1)S(1)}, bf16[192,512]{1,0:T(8,128)(2,1)}, u32[]{:S(2)}) copy-start(bf16[192,512]{1,0:T(8,128)(2,1)} %cot_ref.1) | copy-start | bytes 589828
  0.7 6.0 %copy-start.6 = (f32[192,2]{0,1:T(2,128)S(1)}, f32[192,2]{0,1:T(2,128)}, u32[]{:S(2)}) copy-start(f32[192,2]{0,1:T(2,128)} %param.17) | copy-start | bytes 4612
  3.7 4.6 %copy-start.14 = (bf16[192,512]{1,0:T(8,128)(2,1)S(1)}, bf16[192,512]{1,0:T(8,128)(2,1)}, u32[]{:S(2)}) copy-start(bf16[192,512]{1,0:T(8,128)(2,1)} %param.14) | copy-start | bytes 589828
  52.5 5.5 %copy-start.9 = (bf16[1,2048,896]{2,1,0:T(8,128)(2,1)S(1)}, bf16[1,2048,896]{2,1,0:T(8,128)(2,1)}, u32[]{:S(2)}) copy-start(bf16[1,2048,896]{2,1,0:T(8,128)(2,1)} %param.19) | copy-start | bytes 11010052
  52.5 5.5 %copy-start.10 = (bf16[8,72,2048]{2,1,0:T(8,128)(2,1)S(1)}, bf16[8,72,2048]{2,1,0:T(8,128)(2,1)}, u32[]{:S(2)}) copy-start(bf16[8,72,2048]{2,1,0:T(8,128)(2,1)} %get-tuple-element.12) | copy-start | bytes 7077892
  58.0 2.7 %copy-start.17 = (f32[576,896]{1,0:T(8,128)}, f32[576,896]{1,0:T(8,128)S(1)}, u32[]{:S(2)}) copy-start(f32[576,896]{1,0:T(8,128)S(1)} %fusion.2) | copy-start | bytes 6193156
  58.1 2.8 %copy-start.7 = (bf16[1,896,2048]{2,1,0:T(8,128)(2,1)S(1)}, bf16[1,896,2048]{2,1,0:T(8,128)(2,1)}, u32[]{:S(2)}) copy-start(bf16[1,896,2048]{2,1,0:T(8,128)(2,1)} %param.20) | copy-start | bytes 11010052
  58.1 3.5 %copy-start.12 = (bf16[8,72,2048]{2,1,0:T(8,128)(2,1)S(1)}, bf16[8,72,2048]{2,1,0:T(8,128)(2,1)}, u32[]{:S(2)}) copy-start(bf16[8,72,2048]{2,1,0:T(8,128)(2,1)} %get-tuple-element.13) | copy-start | bytes 7077892
  60.7 4.1 %copy-start.18 = (f32[576,896]{1,0:T(8,128)}, f32[576,896]{1,0:T(8,128)S(1)}, u32[]{:S(2)}) copy-start(f32[576,896]{1,0:T(8,128)S(1)} %fusion.6) | copy-start | bytes 6193156
  61.6 3.3 %copy-start.8 = (bf16[1,2048,896]{2,1,0:T(8,128)(2,1)S(1)}, bf16[1,2048,896]{2,1,0:T(8,128)(2,1)}, u32[]{:S(2)}) copy-start(bf16[1,2048,896]{2,1,0:T(8,128)(2,1)} %param.18) | copy-start | bytes 11010052
  64.8 2.7 %copy-start.19 = (bf16[576,896]{1,0:T(8,128)(2,1)}, bf16[576,896]{1,0:T(8,128)(2,1)S(1)}, u32[]{:S(2)}) copy-start(bf16[576,896]{1,0:T(8,128)(2,1)S(1)} %get-tuple-element.22) | copy-start | bytes 3096580
  71.4 33.3 %copy-start.15 = (f32[192,256]{1,0:T(8,128)S(1)}, f32[192,256]{1,0:T(8,128)}, u32[]{:S(2)}) copy-start(f32[192,256]{1,0:T(8,128)} %get-tuple-element.14) | copy-start | bytes 589828
  71.4 33.3 %copy-start.16 = (bf16[192,256]{1,0:T(8,128)(2,1)S(1)}, bf16[192,256]{1,0:T(8,128)(2,1)}, u32[]{:S(2)}) copy-start(bf16[192,256]{1,0:T(8,128)(2,1)} %param.23) | copy-start | bytes 294916
  107.4 23.6 %copy-start.2 = (bf16[192,256]{1,0:T(8,128)(2,1)S(1)}, bf16[192,256]{1,0:T(8,128)(2,1)}, u32[]{:S(2)}) copy-start(bf16[192,256]{1,0:T(8,128)(2,1)} %param.22) | copy-start | bytes 294916
  107.4 23.6 %copy-start.4 = (f32[192,256]{1,0:T(8,128)S(1)}, f32[192,256]{1,0:T(8,128)}, u32[]{:S(2)}) copy-start(f32[192,256]{1,0:T(8,128)} %get-tuple-element.17) | copy-start | bytes 589828
  131.0 5.2 %copy-start.13 = (bf16[8,72,2048]{2,1,0:T(8,128)(2,1)S(1)}, bf16[8,72,2048]{2,1,0:T(8,128)(2,1)}, u32[]{:S(2)}) copy-start(bf16[8,72,2048]{2,1,0:T(8,128)(2,1)} %get-tuple-element.13) | copy-start | bytes 7077892
  136.1 7.0 %copy-start.11 = (bf16[8,72,2048]{2,1,0:T(8,128)(2,1)S(1)}, bf16[8,72,2048]{2,1,0:T(8,128)(2,1)}, u32[]{:S(2)}) copy-start(bf16[8,72,2048]{2,1,0:T(8,128)(2,1)} %get-tuple-element.12) | copy-start | bytes 7077892
  136.1 7.0 %copy-start.20 = (bf16[576,896]{1,0:T(8,128)(2,1)S(1)}, bf16[576,896]{1,0:T(8,128)(2,1)}, u32[]{:S(2)}) copy-start(bf16[576,896]{1,0:T(8,128)(2,1)} %copy-done.19) | copy-start | bytes 3096580
  148.0 4.8 %copy-start.3 = (f32[256,256]{1,0:T(8,128)S(1)}, f32[256,256]{1,0:T(8,128)}, u32[]{:S(2)}) copy-start(f32[256,256]{1,0:T(8,128)} %get-tuple-element.41) | copy-start | bytes 786436
where the time goes:
time: 155 us; the launch traced here: 154 us
  Pallas kernels  96.7 us (62%)
  matrix products  46.5 us (30%)
  other arithmetic  7.01 us (5%)
  local copies, waits for them, and re-layouts  2.47 us (2%)
    pallas_call x1, Pallas kernels, dispatch(): pl.pallas_call(functools.partial(dispatch_kernel, n, m), out_shape=(whole...  43.1 us
    pallas_call x1, Pallas kernels, bring_back(): pl.pallas_call(functools.partial(return_kernel, n, m), out_shape=jax.Shap...  32.3 us
    pallas_call x1, Pallas kernels, tail(): pl.pallas_call(functools.partial(tail_kernel, n), out_shape=(jax.ShapeDty...  21.2 us
    dot_general x1, matrix products, expert_backward(): lax.dot_general(hidden, cotangent, (((0,), (0,)), ((), ())), preferred_el...  7.02 us
    dot_general x1, matrix products, expert_backward(): gate_act = jnp.dot(inputs, gate_weight, preferred_element_type=jnp.float32)  5.49 us
    dot_general x1, matrix products, expert_backward(): lax.dot_general(inputs, d_up, (((0,), (0,)), ((), ())), preferred_element...  4.84 us
    dot_general x1, matrix products, expert_backward(): lax.dot_general(inputs, d_gate, (((0,), (0,)), ((), ())), preferred_eleme...  4.84 us
    dot_general x1, matrix products, expert_backward(): lax.dot_general(d_up, up_weight, (((1,), (1,)), ((), ())), preferred_elem...  3.89 us

commit v1 on v0

v1 whole, which is shorter than its diff:
```python
import functools

import jax
import jax.numpy as jnp
from jax import lax
from jax.experimental import pallas as pl
from jax.experimental.pallas import tpu as pltpu
from jax.sharding import PartitionSpec as P

MESH = pl.DeviceIdType.MESH


def partner(t, stage, m):
    d = m >> (stage + 1)
    return t + d * (1 - 2 * ((t // d) % 2))


def flipped(s, j, n):
    out = 0
    for b in range(n.bit_length() - 1):
        bit = (s // 2**b) % 2
        out = out + (1 - bit if (j >> b) % 2 else bit) * 2**b
    return out


def far_near(n):
    near, far = list(range(n // 2)), list(range(n // 2, n))
    arrive = near[:1]
    for i in range(1, n // 2):
        arrive += [near[i], far[i - 1]]
    leave = []
    for i in range(1, n // 2):
        leave += [far[i - 1], near[i]]
    return arrive + far[-1:], leave + far[-1:], far + near[1:] + near[:1]


def held_columns(t, stage, m):
    if stage == 0:
        return [t]
    return held_columns(t, stage - 1, m) + held_columns(partner(t, stage - 1, m), stage - 1, m)


def greet(peers):
    barrier = pltpu.get_barrier_semaphore()
    for peer in peers:
        pl.semaphore_signal(barrier, inc=1, device_id=peer, device_id_type=MESH)
    pl.semaphore_wait(barrier, len(peers))


def remote(src, dst, send_sem, recv_sem, peer):
    return pltpu.make_async_remote_copy(
        src_ref=src,
        dst_ref=dst,
        send_sem=send_sem,
        recv_sem=recv_sem,
        device_id=peer,
        device_id_type=MESH,
    )


def shifted(value, k, fill, reverse):
    pad = jnp.full((k, value.shape[1]), fill, value.dtype)
    if reverse:
        return jnp.concatenate([value[k:], pad], axis=0)
    return jnp.concatenate([pad, value[:-k]], axis=0)


def local_scan(gain, term, reverse):
    k = 1
    while k < gain.shape[0]:
        term = term + gain * shifted(term, k, 0.0, reverse)
        gain = gain * shifted(gain, k, 1.0, reverse)
        k *= 2
    return gain, term


def dispatch_kernel(
    n,
    m,
    rows_ref,
    cot_ref,
    decay_ref,
    driven_ref,
    rows_out,
    cot_out,
    states_ref,
    prev_ref,
    gain_buf,
    car_send,
    car_buf,
    a2a_send,
    a2a_recv,
    tp_send,
    tp_recv,
    car_ssem,
    car_rsem,
    self_sem,
):
    sources, targets = (rows_ref, cot_ref), (rows_out, cot_out)
    s, t = lax.axis_index("sp"), lax.axis_index("tp")
    feat = rows_ref.shape[2]
    stages = m.bit_length() - 1
    greet(
        [{"sp": lax.rem(s + k, n)} for k in range(1, n)]
        + [{"tp": partner(t, j, m)} for j in range(stages)]
    )

    def block(a, src, col):
        return targets[a].at[src, :, pl.ds(pl.multiple_of(col * feat, feat), feat)]

    first = {}
    arrive, leave, _ = far_near(n)
    for k in [0] + leave:
        dst = flipped(s, k, n)
        for a in range(2):
            if k == 0:
                copy = pltpu.make_async_copy(sources[a].at[s], block(a, s, t), self_sem.at[a])
            else:
                copy = remote(
                    sources[a].at[dst],
                    block(a, s, t),
                    a2a_send.at[a, k],
                    a2a_recv.at[a, k],
                    {"sp": dst},
                )
            copy.start()
            first[k, a] = copy

    pushed = []

    def push(a, k, stage, i, col):
        src = flipped(s, k, n)
        at = 2**stage - 1 + i
        copy = remote(
            block(a, src, col),
            block(a, src, col),
            tp_send.at[a, at, k],
            tp_recv.at[a, at, k],
            {"tp": partner(t, stage, m)},
        )
        copy.start()
        pushed.append(copy)

    def arrived(k, stage):
        src = flipped(s, k, n)
        cols = held_columns(partner(t, stage, m), stage, m)
        for i, col in enumerate(cols):
            at = 2**stage - 1 + i
            for a in range(2):
                remote(
                    block(a, src, col),
                    block(a, src, col),
                    tp_send.at[a, at, k],
                    tp_recv.at[a, at, k],
                    {"tp": partner(t, stage, m)},
                ).wait_recv()
                for later in range(stage + 1, stages):
                    push(a, k, later, 2**stage + i, col)

    def forward(k):
        for a in range(2):
            if k == 0:
                first[k, a].wait()
            else:
                first[k, a].wait_recv()
            for stage in range(stages):
                push(a, k, stage, 0, t)

    forward(arrive[0])
    gain, term = local_scan(decay_ref[...], driven_ref[...], False)
    gain_buf[...] = gain
    states_ref[...] = term
    rows = gain.shape[0]
    car_send[0:1] = gain[rows - 1 : rows]
    car_send[1:2] = term[rows - 1 : rows]
    forward(arrive[1])
    carries = []
    for k in range(1, n):
        copy = remote(
            car_send, car_buf.at[k], car_ssem.at[k], car_rsem.at[k], {"sp": lax.rem(s + k, n)}
        )
        copy.start()
        carries.append(copy)
    for at in range(2, n):
        forward(arrive[at])
        for stage in range(stages - 1):
            arrived(arrive[at - 2], stage)
    for copy in carries:
        copy.wait()
    carry = jnp.zeros((1, gain_buf.shape[1]), jnp.float32)
    for k in range(n - 1, 0, -1):
        carry = jnp.where(k <= s, car_buf[k, 0:1] * carry + car_buf[k, 1:2], carry)
    states = states_ref[...] + gain_buf[...] * carry
    states_ref[...] = states
    prev_ref[...] = jnp.concatenate([carry, states[:-1]], axis=0)
    for k in arrive[n - 2 :]:
        for stage in range(stages - 1):
            arrived(k, stage)
    for k in range(n):
        arrived(k, stages - 1)
    for k in leave:
        for a in range(2):
            first[k, a].wait_send()
    for copy in pushed:
        copy.wait_send()


def dispatch(send_rows, send_cot, decay, driven):
    n, m = lax.axis_size("sp"), lax.axis_size("tp")
    _, cap, feat = send_rows.shape
    whole = jax.ShapeDtypeStruct((n, cap, m * feat), send_rows.dtype)
    rows, channels = decay.shape
    vmem = pl.BlockSpec(memory_space=pltpu.VMEM)
    state = jax.ShapeDtypeStruct((rows, channels), jnp.float32)
    return pl.pallas_call(
        functools.partial(dispatch_kernel, n, m),
        out_shape=(whole, whole, state, state),
        in_specs=[vmem] * 4,
        out_specs=(vmem,) * 4,
        scratch_shapes=[
            pltpu.VMEM((rows, channels), jnp.float32),
            pltpu.VMEM((2, channels), jnp.float32),
            pltpu.VMEM((n, 2, channels), jnp.float32),
            pltpu.SemaphoreType.DMA((2, n)),
            pltpu.SemaphoreType.DMA((2, n)),
            pltpu.SemaphoreType.DMA((2, m - 1, n)),
            pltpu.SemaphoreType.DMA((2, m - 1, n)),
            pltpu.SemaphoreType.DMA((n,)),
            pltpu.SemaphoreType.DMA((n,)),
            pltpu.SemaphoreType.DMA((2,)),
        ],
        compiler_params=pltpu.CompilerParams(collective_id=0, has_side_effects=True),
        name="dispatch",
    )(send_rows, send_cot, decay, driven)


def gelu_parts(logits):
    x = logits.astype(jnp.float32)
    square = x * x
    slope = 0.7978845608028654
    th = jnp.tanh(slope * (x + 0.044715 * (x * square)))
    value = 0.5 * x * (1.0 + th)
    inner = slope * (1.0 + 3.0 * 0.044715 * square)
    return value, 0.5 * (1.0 + th) + 0.5 * x * (1.0 - th * th) * inner


def dot_f32(a, b):
    return jnp.dot(a, b, preferred_element_type=jnp.float32)


def dot_rows(a, b):
    return lax.dot_general(
        a, b, (((0,), (0,)), ((), ())), preferred_element_type=jnp.float32
    )


def dot_cols(a, b):
    return lax.dot_general(
        a, b, (((1,), (1,)), ((), ())), preferred_element_type=jnp.float32
    )


def expert_kernel(
    n,
    m,
    x_hbm,
    c_hbm,
    wg_hbm,
    wu_hbm,
    wd_hbm,
    wo_hbm,
    pick_ref,
    cot_ref,
    states_ref,
    prev_ref,
    decay_ref,
    forget_ref,
    admit_ref,
    scale_ref,
    u_ref,
    logits_ref,
    base_ref,
    rw_ref,
    aw_ref,
    gg_ref,
    gu_ref,
    gd_ref,
    gop_ref,
    gin_ref,
    ggp_ref,
    x_ref,
    c_ref,
    wg_ref,
    wu_ref,
    wd_ref,
    wo_ref,
    hid_ref,
    dg_ref,
    du_ref,
    part_ref,
    acc_ref,
    in_buf,
    home_buf,
    back_buf,
    resid_ref,
    lru_ref,
    blk_ref,
    gop_buf,
    val_ref,
    gains_ref,
    full_gain,
    term_ref,
    co_state,
    co_in,
    co_recall,
    co_admit,
    co_direct,
    car_send,
    car_buf,
    ld_sem,
    rs_send,
    rs_recv,
    a2a_send,
    a2a_recv,
    ag_send,
    ag_recv,
    up_send,
    up_recv,
    dn_send,
    dn_recv,
    lo_send,
    lo_recv,
    blk_send,
    blk_recv,
    bt_send,
    bt_recv,
    car_ssem,
    car_rsem,
):
    s, t = lax.axis_index("sp"), lax.axis_index("tp")
    stages = m.bit_length() - 1
    groups = n // 2
    hi, lo = s // 2, s % 2
    other = 1 - lo
    group_rows = x_ref.shape[0] // groups
    cap = group_rows // 2
    width = x_ref.shape[1]
    hidden = hid_ref.shape[1]
    rows, feat = cot_ref.shape
    channels = states_ref.shape[1]
    quarter = rows // m

    def across(stage):
        d = 2**stage
        return t + d * (1 - 2 * ((t // d) % 2))

    def cols(col):
        return pl.ds(pl.multiple_of(col * feat, feat), feat)

    def at_group(q):
        return pl.ds(pl.multiple_of(q * group_rows, 16), group_rows)

    def at_rows(src):
        return pl.ds(pl.multiple_of(src * rows, 16), rows)

    order = [groups - 1 - j for j in range(groups)]
    place = [flipped(hi, f, groups) for f in order]

    loads = {}

    def load(name, src, dst, at):
        copy = pltpu.make_async_copy(src, dst, ld_sem.at[at])
        copy.start()
        loads[name] = copy

    for j in range(groups):
        load(("x", j), x_hbm.at[at_group(place[j])], x_ref.at[at_group(place[j])], j)
        if j == 0:
            load("g", wg_hbm, wg_ref, 2 * groups)
            load("u", wu_hbm, wu_ref, 2 * groups + 1)
            load(("c", 0), c_hbm.at[at_group(place[0])], c_ref.at[at_group(place[0])], groups)
            load("d", wd_hbm, wd_ref, 2 * groups + 2)
        else:
            load(("c", j), c_hbm.at[at_group(place[j])], c_ref.at[at_group(place[j])], groups + j)
    load("o", wo_hbm, wo_ref, 2 * groups + 3)

    greet(
        [{"sp": lax.rem(s + k, n)} for k in range(1, n)] + [{"tp": across(j)} for j in range(stages)]
    )

    gelu_val, gelu_der = gelu_parts(logits_ref[...])
    states = states_ref[...]
    lru_ref[at_rows(s), :] = (states * gelu_val).astype(jnp.bfloat16)
    co_in[...] = gelu_val
    co_state[...] = states * gelu_der

    def line(step, up):
        src = hi - step if up else hi + step
        block = at_rows(src * 2 + lo)
        peer = hi + 1 if up else hi - 1
        return remote(
            lru_ref.at[block],
            lru_ref.at[block],
            (up_send if up else dn_send).at[step],
            (up_recv if up else dn_recv).at[step],
            {"sp": peer * 2 + lo},
        )

    def beside(src_hi):
        block = at_rows(src_hi * 2 + lo)
        return remote(
            lru_ref.at[block],
            lru_ref.at[block],
            lo_send.at[src_hi],
            lo_recv.at[src_hi],
            {"sp": hi * 2 + other},
        )

    def line_send(step):
        @pl.when((hi >= step) & (hi < groups - 1))
        def _():
            line(step, True).start()

        @pl.when((hi + step < groups) & (hi > 0))
        def _():
            line(step, False).start()

    def line_step(step):
        @pl.when(hi > step)
        def _():
            line(step, True).wait_recv()
            beside(hi - 1 - step).start()

        @pl.when(hi + step < groups - 1)
        def _():
            line(step, False).wait_recv()
            beside(hi + 1 + step).start()

        if step + 1 < groups - 1:
            line_send(step + 1)

    def line_end():
        for step in range(groups - 1):
            @pl.when((hi >= step) & (hi < groups - 1))
            def _():
                line(step, True).wait_send()

            @pl.when((hi + step < groups) & (hi > 0))
            def _():
                line(step, False).wait_send()

        for src_hi in range(groups):
            beside(src_hi).wait()

    line_send(0)
    beside(hi).start()

    base = []
    total = 0
    for stage in range(stages):
        base.append(total)
        total += m >> (stage + 1)
    waits = []

    def send_stage(q, stage):
        source = part_ref if stage == 0 else acc_ref
        step = 2 ** (stage + 1)
        for i in range(m // step):
            col = lax.rem(across(stage) + i * step, m)
            copy = stage_copy(q, stage, i, col, source)
            copy.start()
            waits.append(copy)

    def stage_copy(q, stage, i, col, source):
        at = base[stage] + i
        return remote(
            source.at[at_group(q), cols(col)],
            in_buf.at[at, q],
            rs_send.at[at, q],
            rs_recv.at[at, q],
            {"tp": across(stage)},
        )

    def sum_stage(q, stage):
        source = part_ref if stage == 0 else acc_ref
        step = 2 ** (stage + 1)
        value = None
        for i in range(m // step):
            col = lax.rem(t + i * step, m)
            stage_copy(q, stage, i, col, source).wait_recv()
            value = source[at_group(q), cols(col)].astype(jnp.float32)
            value = value + in_buf[base[stage] + i, q].astype(jnp.float32)
            if stage + 1 < stages:
                acc_ref[at_group(q), cols(col)] = value.astype(jnp.bfloat16)
        return value

    def home_copy(k):
        dst = flipped(s, k, n)
        return remote(
            home_buf.at[dst], back_buf.at[s], a2a_send.at[k], a2a_recv.at[k], {"sp": dst}
        )

    def middle(j):
        for stage in range(stages - 1):
            sum_stage(place[j], stage)
            send_stage(place[j], stage + 1)

    def finish(j):
        value = sum_stage(place[j], stages - 1)
        q = place[j]
        for half in range(2):
            home_buf[2 * q + half] = value[half * cap : (half + 1) * cap].astype(jnp.bfloat16)
        for k in (2 * order[j], 2 * order[j] + 1):
            if k > 0:
                copy = home_copy(k)
                copy.start()
                waits.append(copy)

    tile = 256
    cuts = [(f, min(tile, hidden - f)) for f in range(0, hidden, tile)]

    def forward(j):
        block = at_group(place[j])
        for f0, size in cuts:
            f = pl.ds(f0, size)
            if j == 0 and f0 == 0:
                loads["x", 0].wait()
                loads["g"].wait()
            gate_act = dot_f32(x_ref[block, :], wg_ref[:, f])
            if j == 0 and f0 == 0:
                loads["u"].wait()
            up_act = dot_f32(x_ref[block, :], wu_ref[:, f])
            if j == 0 and f0 == 0:
                loads["c", 0].wait()
                loads["d"].wait()
            d_hidden = dot_cols(c_ref[block, :], wd_ref[f, :])
            sig = jax.nn.sigmoid(gate_act)
            silu = gate_act * sig
            hid_ref[block, f] = (silu * up_act).astype(jnp.bfloat16)
            du_ref[block, f] = (d_hidden * silu).astype(jnp.bfloat16)
            dg_ref[block, f] = (
                d_hidden * up_act * sig * (1.0 + gate_act * (1.0 - sig))
            ).astype(jnp.bfloat16)

    def partial(j, first, last):
        block = at_group(place[j])

        def body(i, carry):
            step = i // (m // 2)
            col = lax.rem(across(0) + step * (t - across(0)) + 2 * lax.rem(i, m // 2) + m, m)
            value = dot_cols(dg_ref[block, :], wg_ref[cols(col), :])
            value = value + dot_cols(du_ref[block, :], wu_ref[cols(col), :])
            part_ref[block, cols(col)] = value.astype(jnp.bfloat16)
            return carry

        lax.fori_loop(first, last, body, 0)

    for j in range(groups):
        if j > 0:
            loads["x", j].wait()
            loads["c", j].wait()
        forward(j)
        if j < groups - 1:
            line_step(j)
        if j > 0:
            middle(j - 1)
        if j > 1:
            finish(j - 2)
        partial(j, 0, m // 2)
        send_stage(place[j], 0)
        partial(j, m // 2, m)

    x_tiles = width // tile
    h_tiles = hidden // 128
    work = [("x", i) for i in range(x_tiles)] + [("h", i) for i in range(h_tiles)]
    done = [0]

    def x_body(i, carry):
        c = pl.ds(pl.multiple_of(i * tile, tile), tile)
        left = x_ref[:, c]
        gg_ref[c, :] = dot_rows(left, dg_ref[...]).astype(jnp.bfloat16)
        gu_ref[c, :] = dot_rows(left, du_ref[...]).astype(jnp.bfloat16)
        return carry

    def h_body(i, carry):
        c = pl.ds(pl.multiple_of(i * 128, 128), 128)
        gd_ref[c, :] = dot_rows(hid_ref[:, c], c_ref[...]).astype(jnp.bfloat16)
        return carry

    def weight_tiles(count):
        stop = min(done[0] + count, x_tiles + h_tiles)
        x_stop = min(stop, x_tiles)
        if done[0] < x_stop:
            lax.fori_loop(done[0], x_stop, x_body, 0)
            done[0] = x_stop
        if done[0] < stop:
            lax.fori_loop(done[0] - x_tiles, stop - x_tiles, h_body, 0)
            done[0] = stop

    last = groups - 1
    weight_tiles(1)
    middle(last)
    if last > 0:
        finish(last - 1)
    decay = decay_ref[...]
    gain = shifted(decay, 1, 1.0, True)
    k = 1
    step = 0
    while k < rows:
        gains_ref[step] = gain
        gain = gain * shifted(gain, k, 1.0, True)
        k *= 2
        step += 1
    full_gain[...] = gain
    forget = forget_ref[...]
    admit = admit_ref[...]
    scale = scale_ref[...]
    u = u_ref[...].astype(jnp.float32)
    co_direct[...] = admit * scale
    co_admit[...] = u * scale * admit * (1.0 - admit)
    d_log = prev_ref[...] * decay - u * admit * decay * decay / scale
    co_recall[...] = d_log * (-8.0 * base_ref[...]) * forget * (1.0 - forget)
    weight_tiles(2)
    finish(last)
    val_ref[...] = cot_ref[...].astype(jnp.float32)

    def collect(k):
        src = flipped(s, k, n)
        if k > 0:
            home_copy(k).wait_recv()
            part = back_buf[src]
        else:
            part = home_buf[s]
        val_ref[...] += dot_f32(pick_ref[src], part)

    for k in range(n - 1, 3, -1):
        collect(k)
    weight_tiles(1)
    for k in range(min(3, n - 1), -1, -1):
        collect(k)
    resid_ref[:, cols(t)] = val_ref[...].astype(jnp.bfloat16)

    def share(stage, i, col):
        at = 2**stage - 1 + i
        return remote(
            resid_ref.at[:, cols(col)],
            resid_ref.at[:, cols(col)],
            ag_send.at[at],
            ag_recv.at[at],
            {"tp": partner(t, stage, m)},
        )

    def push(stage, i, col):
        copy = share(stage, i, col)
        copy.start()
        waits.append(copy)

    for stage in range(stages):
        push(stage, 0, t)
    weight_tiles(5)
    for stage in range(stages):
        for i, col in enumerate(held_columns(partner(t, stage, m), stage, m)):
            share(stage, i, col).wait_recv()
            for later in range(stage + 1, stages):
                push(later, 2**stage + i, col)

    bw = blk_ref.shape[1]
    own = width // n

    def block_cols(index):
        return pl.ds(pl.multiple_of(index * own // bw * bw, bw), bw)

    def piece(src, at):
        start = src * rows + at * quarter
        return pl.ds(pl.multiple_of(start, 16), quarter)

    def block_copy(k):
        dst = flipped(s, k, n)
        return remote(
            resid_ref.at[pl.ds(pl.multiple_of(t * quarter, 16), quarter), block_cols(dst)],
            blk_ref.at[piece(s, t)],
            blk_send.at[k],
            blk_recv.at[k],
            {"sp": dst},
        )

    def pass_copy(k, stage, i, at):
        src = flipped(s, k, n)
        spot = 2**stage - 1 + i
        return remote(
            blk_ref.at[piece(src, at)],
            blk_ref.at[piece(src, at)],
            bt_send.at[spot, k],
            bt_recv.at[spot, k],
            {"tp": partner(t, stage, m)},
        )

    def pass_on(k, stage, i, at):
        copy = pass_copy(k, stage, i, at)
        copy.start()
        waits.append(copy)

    def pass_arrived(k, stage):
        for i, at in enumerate(held_columns(partner(t, stage, m), stage, m)):
            pass_copy(k, stage, i, at).wait_recv()
            for later in range(stage + 1, stages):
                pass_on(k, later, 2**stage + i, at)

    arrive, leave, _ = far_near(n)
    for k in leave:
        copy = block_copy(k)
        copy.start()
        waits.append(copy)
    blk_ref[at_rows(s), :] = resid_ref[:, block_cols(s)]
    loads["o"].wait()
    mixer = dot_f32(resid_ref[...], wo_ref[...])
    ggp_ref[...] = mixer * co_state[...]
    term = mixer * co_in[...]
    k = 1
    step = 0
    while k < rows:
        term = term + gains_ref[step] * shifted(term, k, 0.0, True)
        k *= 2
        step += 1
    term_ref[...] = term
    first_decay = decay_ref[0:1]
    car_send[0:1] = first_decay * full_gain[0:1]
    car_send[1:2] = first_decay * term[0:1]
    carries = []
    for k in range(1, n):
        copy = remote(
            car_send, car_buf.at[k], car_ssem.at[k], car_rsem.at[k], {"sp": lax.rem(s + k, n)}
        )
        copy.start()
        carries.append(copy)
    inbound = arrive[1:]
    for at in range(len(inbound)):
        block_copy(inbound[at]).wait_recv()
        for stage in range(stages):
            pass_on(inbound[at], stage, 0, t)
        if at == len(inbound) // 2:
            weight_tiles(x_tiles + h_tiles)
    line_end()
    for copy in carries:
        copy.wait()
    carry = jnp.zeros((1, channels), jnp.float32)
    for k in range(1, n):
        carry = jnp.where(k > s, car_buf[k, 0:1] * carry + car_buf[k, 1:2], carry)
    for k in inbound:
        for stage in range(stages - 1):
            pass_arrived(k, stage)
    state_grad = term_ref[...] + full_gain[...] * carry
    d_recall = (state_grad * co_recall[...]).astype(jnp.bfloat16)
    d_admit = (state_grad * co_admit[...]).astype(jnp.bfloat16)
    direct = state_grad * co_direct[...]
    lane = rw_ref.shape[1]
    local = channels // lane
    for b in range(local):
        c = slice(b * lane, (b + 1) * lane)
        gin_ref[:, c] = (
            direct[:, c]
            + dot_cols(d_recall[:, c], rw_ref[t * local + b])
            + dot_cols(d_admit[:, c], aw_ref[t * local + b])
        )
    for k in inbound:
        pass_arrived(k, stages - 1)
    gop_buf[...] = dot_rows(blk_ref[...], lru_ref[...])
    start = lax.rem(s * own, bw)
    gop_ref[...] = gop_buf[pl.ds(pl.multiple_of(start, 8), own), :]
    for copy in waits:
        copy.wait_send()


def expert_step(rows_in, cot_in, weights, pick, cot, recurrent):
    n, m = lax.axis_size("sp"), lax.axis_size("tp")
    total, width = rows_in.shape
    hidden = weights[2].shape[0]
    rows, feat = cot.shape
    channels = recurrent[0].shape[1]
    cap = total // n
    groups = n // 2
    own = width // n
    bw = max(128, own)
    levels = (rows - 1).bit_length()
    bf16, f32 = jnp.bfloat16, jnp.float32
    vmem = pl.BlockSpec(memory_space=pltpu.VMEM)
    hbm = pl.BlockSpec(memory_space=pl.ANY)
    dma = pltpu.SemaphoreType.DMA
    state = pltpu.VMEM((rows, channels), f32)
    return pl.pallas_call(
        functools.partial(expert_kernel, n, m),
        out_shape=(
            pltpu.VMEM((width, hidden), bf16),
            pltpu.VMEM((width, hidden), bf16),
            pltpu.VMEM((hidden, width), bf16),
            pltpu.VMEM((own, channels), f32),
            pltpu.VMEM((rows, channels), f32),
            pltpu.VMEM((rows, channels), f32),
        ),
        in_specs=[hbm] * 6 + [vmem] * (2 + len(recurrent)),
        out_specs=(vmem,) * 6,
        scratch_shapes=[
            pltpu.VMEM((total, width), bf16),
            pltpu.VMEM((total, width), bf16),
            pltpu.VMEM((width, hidden), bf16),
            pltpu.VMEM((width, hidden), bf16),
            pltpu.VMEM((hidden, width), bf16),
            pltpu.VMEM((width, channels), bf16),
            pltpu.VMEM((total, hidden), bf16),
            pltpu.VMEM((total, hidden), bf16),
            pltpu.VMEM((total, hidden), bf16),
            pltpu.VMEM((total, width), bf16),
            pltpu.VMEM((total, width), bf16),
            pltpu.VMEM((m - 1, groups, 2 * cap, feat), bf16),
            pltpu.VMEM((n, cap, feat), bf16),
            pltpu.VMEM((n, cap, feat), bf16),
            pltpu.VMEM((rows, width), bf16),
            pltpu.VMEM((n * rows, channels), bf16),
            pltpu.VMEM((n * rows, bw), bf16),
            pltpu.VMEM((bw, channels), f32),
            pltpu.VMEM((rows, feat), f32),
            pltpu.VMEM((levels, rows, channels), f32),
            state,
            state,
            state,
            state,
            state,
            state,
            state,
            pltpu.VMEM((2, channels), f32),
            pltpu.VMEM((n, 2, channels), f32),
            dma((2 * groups + 4,)),
            dma((m - 1, groups)),
            dma((m - 1, groups)),
            dma((n,)),
            dma((n,)),
            dma((m - 1,)),
            dma((m - 1,)),
            dma((groups,)),
            dma((groups,)),
            dma((groups,)),
            dma((groups,)),
            dma((groups,)),
            dma((groups,)),
            dma((n,)),
            dma((n,)),
            dma((m - 1, n)),
            dma((m - 1, n)),
            dma((n,)),
            dma((n,)),
        ],
        compiler_params=pltpu.CompilerParams(
            collective_id=1, has_side_effects=True, vmem_limit_bytes=44 * 2**20
        ),
        name="expert_step",
    )(rows_in, cot_in, *weights, pick, cot, *recurrent)


def per_device(
    middle_stream,
    output_gradient,
    routes,
    chosen_expert_weight,
    expert_gate_weight,
    expert_up_weight,
    expert_down_weight,
    recurrent_output_weight,
    recurrence_input,
    output_gate_logits,
    recurrence_gate_weight,
    input_gate_weight,
    channel_decay_param,
    extra_log_decay,
):
    rows_dev = middle_stream.shape[0]
    top_count = routes.shape[1]
    experts = lax.axis_size("sp")
    capacity = -(-3 * top_count * rows_dev // (2 * experts))
    capacity = -(-capacity // 8) * 8
    feat_width = middle_stream.shape[1]
    choice = routes.T
    expert_ids = jnp.arange(experts, dtype=jnp.int32)
    named = [(choice[k][None, :] == expert_ids[:, None]) for k in range(top_count)]
    named_any = sum(part.astype(jnp.bfloat16) for part in named)
    position = jnp.arange(rows_dev, dtype=jnp.int32)
    earlier = (position[:, None] < position[None, :]).astype(jnp.bfloat16)
    rank = jnp.dot(named_any, earlier, preferred_element_type=jnp.float32).astype(jnp.int32)
    slot_ids = jnp.arange(experts * capacity, dtype=jnp.int32)
    picks = []
    for k in range(top_count):
        slot = jnp.sum(
            jnp.where(named[k], rank + expert_ids[:, None] * capacity, 0), axis=0, keepdims=True
        )
        picks.append((slot_ids[:, None] == slot).astype(jnp.bfloat16))
    pick_any = sum(picks)
    pick_both = jnp.concatenate(picks, axis=1)
    pair_cot = (
        chosen_expert_weight.T[:, :, None] * output_gradient.astype(jnp.float32)[None]
    ).astype(jnp.bfloat16)
    pair_cot = pair_cot.reshape(-1, feat_width)
    send_rows = jnp.dot(pick_any, middle_stream, preferred_element_type=jnp.bfloat16)
    send_cot = jnp.dot(pick_both, pair_cot, preferred_element_type=jnp.bfloat16)
    channels = recurrence_input.shape[1]
    block_width = recurrence_gate_weight.shape[1]
    local_blocks = channels // block_width
    first_block = lax.axis_index("tp") * local_blocks
    recall_weight = lax.dynamic_slice_in_dim(recurrence_gate_weight, first_block, local_blocks, 0)
    admit_weight = lax.dynamic_slice_in_dim(input_gate_weight, first_block, local_blocks, 0)
    u_blocks = recurrence_input.reshape(rows_dev, local_blocks, block_width)
    forget_gate = jax.nn.sigmoid(
        jnp.einsum(
            "tnb,nbc->tnc", u_blocks, recall_weight, preferred_element_type=jnp.float32
        ).reshape(rows_dev, channels)
    )
    admit_gate = jax.nn.sigmoid(
        jnp.einsum(
            "tnb,nbc->tnc", u_blocks, admit_weight, preferred_element_type=jnp.float32
        ).reshape(rows_dev, channels)
    )
    baseline_rate = jax.nn.softplus(-channel_decay_param)
    decay_logarithm = -8.0 * forget_gate * baseline_rate[None, :] + extra_log_decay
    decay_step = jnp.exp(decay_logarithm)
    input_scale = jnp.sqrt(-jnp.expm1(2.0 * decay_logarithm))
    u_float = recurrence_input.astype(jnp.float32)
    driven = u_float * admit_gate * input_scale
    recv_rows, recv_cot, states, prev_states = dispatch(
        send_rows.reshape(experts, capacity, feat_width),
        send_cot.reshape(experts, capacity, feat_width),
        decay_step,
        driven,
    )
    row_width = recv_rows.shape[2]
    grads = expert_step(
        recv_rows.reshape(-1, row_width),
        recv_cot.reshape(-1, row_width),
        (expert_gate_weight[0], expert_up_weight[0], expert_down_weight[0], recurrent_output_weight),
        pick_any.reshape(experts, capacity, rows_dev).transpose(0, 2, 1),
        output_gradient,
        (
            states,
            prev_states,
            decay_step,
            forget_gate,
            admit_gate,
            input_scale,
            recurrence_input,
            output_gate_logits,
            baseline_rate[None, :],
            recurrence_gate_weight,
            input_gate_weight,
        ),
    )
    grad_gate, grad_up, grad_down, grad_out_proj, grad_input, grad_gate_pre = grads
    return (
        grad_gate[None],
        grad_up[None],
        grad_down[None],
        grad_out_proj,
        grad_input,
        grad_gate_pre,
    )


def solution(mesh):
    placed = (
        P("sp", "tp"),
        P("sp", "tp"),
        P("sp", None),
        P("sp", None),
        P("sp", None, "tp"),
        P("sp", None, "tp"),
        P("sp", "tp", None),
        P(None, "tp"),
        P("sp", "tp"),
        P("sp", "tp"),
        P(),
        P(),
        P("tp"),
        P("sp", "tp"),
    )
    return jax.shard_map(
        per_device,
        mesh=mesh,
        in_specs=placed,
        out_specs=(
            P("sp", None, "tp"),
            P("sp", None, "tp"),
            P("sp", "tp", None),
            P("sp", "tp"),
            P("sp", "tp"),
            P("sp", "tp"),
        ),
        check_vma=False,
    )
```

time: 155 us -> 122 us (0.79)
  matrix products: 46.5 us -> 4.82 us
  local copies, waits for them, and re-layouts: 2.47 us -> 9.95 us
  Pallas kernels: 96.7 us -> 102 us
  other arithmetic: 7.01 us -> 4.53 us
    dot_general x12 -> x0, matrix products: 41.5 us -> none  [the longest x1 7.02 us: expert_backward(): lax.dot_general(hidden, cotangent, (((0,), (0,)), ((), ())), preferred_el...]
    unnamed x43 -> x12, local copies, waits for them, and re-layouts: 1.67 us -> 7.59 us
    pallas_call x2 -> x1, Pallas kernels: 53.6 us -> 58.6 us  [expert_step(): pl.pallas_call(functools.partial(expert_kernel, n, m), out_shape=(pltpu.V...]
    add x1 -> x0, other arithmetic: 1.74 us -> none  [per_device(): state_grad * admit_gate * input_scale]
where the time goes in v1:
time: 122 us
  Pallas kernels  102 us (84%)
  local copies, waits for them, and re-layouts  9.95 us (8%)
  matrix products  4.82 us (4%)
  other arithmetic  4.53 us (4%)
    pallas_call x1, Pallas kernels, expert_step(): pl.pallas_call(functools.partial(expert_kernel, n, m), out_shape=(pltpu.V...  58.6 us
    pallas_call x1, Pallas kernels, dispatch(): pl.pallas_call(functools.partial(dispatch_kernel, n, m), out_shape=(whole...  43 us
    unnamed x12, local copies, waits for them, and re-layouts  7.59 us

profile of v1, /device:TPU:1, one launch (start us, length us, event | category | flops | bytes accessed | tf_op | source)
XLA Modules:
  0.0 121.7 jit_solution(14870490993150796027)
XLA Ops:
  0.6 0.0 copy-start
  0.6 0.0 copy-start.1
  0.7 0.0 copy-start.2
  0.7 0.8 mul.57
  1.5 0.8 fusion.41
  2.3 0.1 select_reduce_fusion.1
  2.4 1.3 %broadcast_multiply_fusion = (f32[256]{0:T(256)S(1)}, f32[256]{0:T(256)}) fusion(f32[256]{0:T(256)} %param.26), kind=kLoop, calls=%fused_computation.56 | loop fusion | flops 2048 | bytes 3072 | tf_op jit(solution)/shard_map/mul | solution.py:921
  3.7 1.1 fusion.7
  4.8 1.1 fusion.3
  5.9 0.2 broadcast_compare_fusion.1
  6.2 1.0 fusion.16.pick_ref
  7.1 1.0 convert_element_type.41
  8.1 0.1 fusion.13
  8.2 1.3 %fusion.9.cot_ref = bf16[8,72,512]{2,1,0:T(8,128)(2,1)} fusion(pred[8,72,192]{2,1,0:T(8,128)(4,1)S(1)} %get-tuple-element.34, pred[8,72,192]{2,1,0:T(8,128)(4,1)S(1)} %get-tuple-element.33, bf16[384,512]{1,0:T(8,128)(2,1)S(1)} %fusion.13), kind=kOutput, calls=%fused_computation.12 | convolution fusion | flops 226713600 | bytes 1204224 | tf_op jit(solution)/shard_map/dot_general | solution.py:902
  9.6 0.8 copy_bitcast_fusion
  10.3 0.0 copy-done.1
  10.3 0.0 copy-done.2
  10.3 1.0 multiply_multiply_fusion
  11.3 0.0 copy-done
  11.3 1.1 fusion.19
  12.5 43.0 %dispatch.1 = (bf16[8,72,2048]{2,1,0:T(8,128)(2,1)}, bf16[8,72,2048]{2,1,0:T(8,128)(2,1)}, f32[192,256]{1,0:T(8,128)}, f32[192,256]{1,0:T(8,128)}) custom-call(bf16[8,72,512]{2,1,0:T(8,128)(2,1)} %bitcast.59, bf16[8,72,512]{2,1,0:T(8,128)(2,1)} %fusion.9.cot_ref, f32[192,256]{1,0:T(8,128)} %get-tuple-element.32.decay_ref, ...), custom_call_target="tpu_custom_call" | custom-call | tf_op jit(solution)/shard_map/dispatch/pallas_call | solution.py:215
  55.5 58.6 %expert_step.1 = (bf16[2048,896]{1,0:T(8,128)(2,1)S(1)}, bf16[2048,896]{1,0:T(8,128)(2,1)S(1)}, bf16[896,2048]{1,0:T(8,128)(2,1)S(1)}, f32[256,256]{1,0:T(8,128)...) custom-call(bf16[576,2048]{1,0:T(8,128)(2,1)} %bitcast.57, bf16[576,2048]{1,0:T(8,128)(2,1)} %bitcast.58, ...), custom_call_target="tpu_custom_call" | custom-call | tf_op jit(solution)/shard_map/expert_step/pallas_call | solution.py:790
  114.1 1.8 %copy.50 = bf16[1,2048,896]{2,1,0:T(8,128)(2,1)} copy(bf16[1,2048,896]{2,1,0:T(8,128)(2,1)S(1)} %bitcast.53) | data formatting | bytes 7340032
  116.0 1.8 %copy.51 = bf16[1,2048,896]{2,1,0:T(8,128)(2,1)} copy(bf16[1,2048,896]{2,1,0:T(8,128)(2,1)S(1)} %bitcast.52) | data formatting | bytes 7340032
  117.8 0.7 copy.54
  118.5 0.7 copy.55
  119.2 0.7 copy.53
  119.9 1.8 %copy.52 = bf16[1,896,2048]{2,1,0:T(8,128)(2,1)} copy(bf16[1,896,2048]{2,1,0:T(8,128)(2,1)S(1)} %bitcast.51) | data formatting | bytes 7340032
  (2 shorter events, 0.0 us)
Async XLA Ops:
  0.6 10.7 %copy-start = (bf16[192,512]{1,0:T(8,128)(2,1)S(1)}, bf16[192,512]{1,0:T(8,128)(2,1)}, u32[]{:S(2)}) copy-start(bf16[192,512]{1,0:T(8,128)(2,1)} %param.14) | copy-start | bytes 589828
  0.6 9.7 %copy-start.1 = (bf16[192,256]{1,0:T(8,128)(2,1)S(1)}, bf16[192,256]{1,0:T(8,128)(2,1)}, u32[]{:S(2)}) copy-start(bf16[192,256]{1,0:T(8,128)(2,1)} %u_ref.1) | copy-start | bytes 294916
  0.7 9.7 %copy-start.2 = (f32[192,256]{1,0:T(8,128)S(1)}, f32[192,256]{1,0:T(8,128)}, u32[]{:S(2)}) copy-start(f32[192,256]{1,0:T(8,128)} %param.27) | copy-start | bytes 589828
